TPU v7x, 32 devices: a whole 2x2x4 slice. The times are simulated.
32 devices in a mesh: sp: 16 (over z, y, x), tp: 2 (over core).
Axes of the slice: x: 2, y: 2, z: 4, core: 2. Of those that a mesh axis runs over, the one named last changes fastest.
Arguments:
- block_input: bfloat16 [4096, 2048], P('sp'), may hold values from -6 to 6
- queries: bfloat16 [4096, 256], P('sp', 'tp'), may hold values from -13 to 13
- keys: bfloat16 [4096, 256], P('sp', 'tp'), may hold values from -13 to 13
- values: bfloat16 [4096, 512], P('sp', 'tp'), may hold values from -6 to 6
- in_gate: float32 [2, 4096], P('tp', 'sp'), may hold values from -110 to 100
- log_forget: float32 [2, 4096], P('tp', 'sp'), may hold values from -0.08 to 0
- grad_out: bfloat16 [4096, 512], P('sp', 'tp'), may hold values from -6 to 6
Outputs:
- grad_queries: bfloat16 [4096, 256], P('sp', 'tp')
- grad_keys: bfloat16 [4096, 256], P('sp', 'tp')
- grad_values: bfloat16 [4096, 512], P('sp', 'tp')
- grad_in_gate: float32 [2, 4096], P('tp', 'sp')
- grad_log_forget: float32 [2, 4096], P('tp', 'sp')
- grad_query_weight: float32 [2048, 256], P('sp', 'tp')
All inputs are finite; a program needn't handle non-finite values.
Results may differ from a plain program's by a relative error of at most 0.012.
The roundings to bfloat16 on the way count: a program that leaves them out, or rounds other values in their place, can miss the bound.
Values sent between devices are 32-bit elements.
A program may use at most 64 MiB of HBM per device.

v0:
```python
import jax
import jax.numpy as jnp
from jax import lax
from jax.sharding import PartitionSpec as P

VERY_LOW = -1e30
EXACT_MODE = lax.Precision.HIGHEST


def carried_in(part, axis, combine, identity, reverse):
    count = lax.axis_size(axis)
    place = lax.axis_index(axis)
    ahead = count - 1 - place if reverse else place
    gathered = jax.tree.map(lambda a: lax.all_gather(a, axis), part)
    state = jax.tree.map(lambda a, e: jnp.zeros_like(a) + jnp.asarray(e, a.dtype), part, identity)

    def one(lap, state):
        source = count - 1 - lap if reverse else lap
        return combine(
            state, jax.tree.map(lambda a: lax.dynamic_index_in_dim(a, source, 0, False), gathered)
        )

    return lax.fori_loop(0, ahead, one, state)


def join_forward(earlier, latter):
    earlier_sum, earlier_max, earlier_mat, earlier_vec = earlier
    latter_sum, latter_max, latter_mat, latter_vec = latter
    new_max = jnp.maximum(latter_sum + earlier_max, latter_max)
    keep_factor = jnp.exp(latter_sum + earlier_max - new_max)
    fresh_factor = jnp.exp(latter_max - new_max)
    return (
        earlier_sum + latter_sum,
        new_max,
        keep_factor[:, None, None] * earlier_mat + fresh_factor[:, None, None] * latter_mat,
        keep_factor[:, None] * earlier_vec + fresh_factor[:, None] * latter_vec,
    )


def join_back(earlier, latter):
    earlier_decay, earlier_mat, earlier_vec = earlier
    latter_decay, latter_mat, latter_vec = latter
    keep_factor = jnp.exp(latter_decay)
    return (
        earlier_decay + latter_decay,
        latter_mat + keep_factor[:, None, None] * earlier_mat,
        latter_vec + keep_factor[:, None] * earlier_vec,
    )


def add_tails(earlier, latter):
    return earlier + latter


def on_device(block_input, queries, keys, values, in_gate, log_forget, grad_out):
    head_count = in_gate.shape[0]
    length = in_gate.shape[1]
    key_size = queries.shape[1] // head_count
    value_size = values.shape[1] // head_count
    scale_of_keys = key_size ** (-0.5)
    row_queries = queries.reshape(length, head_count, key_size)
    key_rows = keys.reshape(length, head_count, key_size)
    row_values = values.reshape(length, head_count, value_size)
    grad_rows = grad_out.reshape(length, head_count, value_size)
    broad_query = row_queries.astype(jnp.float32)
    broad_key = key_rows.astype(jnp.float32)
    broad_value = row_values.astype(jnp.float32)
    forget_sum = jnp.cumsum(log_forget, axis=1)
    block_total = forget_sum[:, -1]
    log_tail = block_total[:, None] - forget_sum + in_gate
    seg_max = jnp.max(log_tail, axis=1)
    factor = jnp.exp(log_tail - seg_max[:, None])
    weighted_terms = (key_rows * factor.T[:, :, None]).astype(jnp.bfloat16)
    segment_matrix = scale_of_keys * jnp.einsum(
        "uae,uap->aep", weighted_terms, row_values, preferred_element_type=jnp.float32
    )
    seg_vec = scale_of_keys * jnp.sum(weighted_terms.astype(jnp.float32), axis=0)
    zero_head = jnp.zeros((head_count,), jnp.float32)
    zero_mat = jnp.zeros((head_count, key_size, value_size), jnp.float32)
    zero_vec = jnp.zeros((head_count, key_size), jnp.float32)
    low_head = jnp.full((head_count,), VERY_LOW, jnp.float32)
    carried = carried_in(
        (block_total, seg_max, segment_matrix, seg_vec),
        "sp",
        join_forward,
        (zero_head, low_head, zero_mat, zero_vec),
        False,
    )
    enter_max, enter_mat, incoming_vector = (carried[1], carried[2], carried[3])
    row_index = lax.broadcasted_iota(jnp.int32, (length, length), 0)
    col_index = lax.broadcasted_iota(jnp.int32, (length, length), 1)
    causal = col_index <= row_index
    log_intra = jnp.where(
        causal[None],
        forget_sum[:, :, None] - forget_sum[:, None, :] + in_gate[:, None, :],
        -jnp.inf,
    )
    intra_max = jnp.max(log_intra, axis=2)
    log_inter = forget_sum + enter_max[:, None]
    row_max = jnp.maximum(log_inter, intra_max)
    inter_weight = jnp.exp(log_inter - row_max)
    intra_weight = jnp.exp(log_intra - row_max[:, :, None])
    column_between = inter_weight.T[:, :, None]
    scores = scale_of_keys * jnp.einsum(
        "thk,shk->hts", row_queries, key_rows, preferred_element_type=jnp.float32
    )
    weighted_scores = intra_weight * scores
    lowered_score = weighted_scores.astype(jnp.bfloat16)
    incoming_lowered = enter_mat.astype(jnp.bfloat16)
    ratio_top = column_between * jnp.einsum(
        "rpn,pns->rps", row_queries, incoming_lowered, preferred_element_type=jnp.float32
    ) + jnp.einsum("ynr,ryp->nyp", lowered_score, row_values, preferred_element_type=jnp.float32)
    denominator = inter_weight * jnp.einsum(
        "thk,hk->ht", broad_query, incoming_vector, precision=EXACT_MODE
    ) + jnp.sum(weighted_scores, axis=2)
    floor_scale = jnp.sqrt(denominator * denominator + jnp.exp(-2.0 * row_max))
    delta_full = grad_rows / floor_scale.T[:, :, None]
    lowered_delta = delta_full.astype(jnp.bfloat16)
    small_offset = -jnp.sum(grad_rows * ratio_top, axis=2).T * denominator / floor_scale**3
    errors = (
        jnp.einsum("thv,shv->hts", lowered_delta, row_values, preferred_element_type=jnp.float32)
        + small_offset[:, :, None]
    )
    backward_lowered = (intra_weight * errors).astype(jnp.bfloat16)
    query_gradient = scale_of_keys * jnp.einsum(
        "flu,ufn->lfn", backward_lowered, key_rows, preferred_element_type=jnp.float32
    ) + column_between * (
        jnp.einsum(
            "ojz,jlz->ojl", lowered_delta, incoming_lowered, preferred_element_type=jnp.float32
        )
        + small_offset.T[:, :, None] * incoming_vector[None]
    )
    grad_low = query_gradient.astype(jnp.bfloat16).reshape(length, head_count * key_size)
    full_term = lax.dot_general(
        block_input, grad_low, (((0,), (0,)), ((), ())), preferred_element_type=jnp.float32
    )
    weight_grad = lax.psum_scatter(full_term, "sp", scatter_dimension=0, tiled=True)
    leave_max = jnp.maximum(block_total + enter_max, seg_max)
    back_decay = block_total + enter_max - leave_max
    query_backward = (row_queries * column_between).astype(jnp.bfloat16)
    backward_matrix = jnp.einsum(
        "url,urg->rlg", query_backward, lowered_delta, preferred_element_type=jnp.float32
    )
    back_vec = jnp.einsum(
        "ht,thk->hk", small_offset * inter_weight, broad_query, precision=EXACT_MODE
    )
    column_decay = jnp.exp(log_tail - leave_max[:, None]).T[:, :, None]
    key_intra = scale_of_keys * jnp.einsum(
        "cov,ocx->vcx", backward_lowered, row_queries, preferred_element_type=jnp.float32
    )
    row_part = jnp.sum(broad_query * query_gradient, axis=2).T
    joined = carried_in(
        (back_decay, backward_matrix, back_vec),
        "sp",
        join_back,
        (zero_head, zero_mat, zero_vec),
        True,
    )
    outgoing_matrix, outgoing_vector = (joined[1], joined[2])
    key_gradient = key_intra + scale_of_keys * column_decay * (
        jnp.einsum("rxi,xei->rxe", broad_value, outgoing_matrix, precision=EXACT_MODE)
        + outgoing_vector[None]
    )
    value_gradient = jnp.einsum(
        "zrf,rzp->fzp", lowered_score, lowered_delta, preferred_element_type=jnp.float32
    ) + scale_of_keys * column_decay * jnp.einsum(
        "brz,rzf->brf", broad_key, outgoing_matrix, precision=EXACT_MODE
    )
    grad_gate = jnp.sum(broad_key * key_gradient, axis=2).T
    forget_part = row_part - grad_gate
    inside = jnp.cumsum(forget_part, axis=1)
    part_total = inside[:, -1]
    suffix = part_total[:, None] - inside + forget_part
    tail_sum = carried_in(part_total, "sp", add_tails, zero_head, True)
    grad_forget = suffix + tail_sum[:, None]
    return (
        grad_low,
        key_gradient.astype(jnp.bfloat16).reshape(length, head_count * key_size),
        value_gradient.astype(jnp.bfloat16).reshape(length, head_count * value_size),
        grad_gate,
        grad_forget,
        weight_grad,
    )


def solution(mesh):
    in_specs = (
        P("sp", None),
        P("sp", "tp"),
        P("sp", "tp"),
        P("sp", "tp"),
        P("tp", "sp"),
        P("tp", "sp"),
        P("sp", "tp"),
    )
    out_specs = (
        P("sp", "tp"),
        P("sp", "tp"),
        P("sp", "tp"),
        P("tp", "sp"),
        P("tp", "sp"),
        P("sp", "tp"),
    )
    return jax.shard_map(
        on_device, mesh=mesh, in_specs=in_specs, out_specs=out_specs, check_vma=False
    )
```

profile of v0, /device:TPU:0, one launch (start us, length us, event | category | flops | bytes accessed | tf_op | source)
XLA Modules:
  0.0 406.7 jit_solution(2943366407485644846)
XLA Ops:
  7.3 1.1 reduce-window.14
  9.4 0.9 copy.33
  10.4 2.0 fusion.56
  12.9 1.8 convolution_multiply_fusion.3
  14.8 1.0 copy.35
  15.8 0.9 copy.37
  16.7 1.2 dynamic-slice
  18.0 1.3 bitcast_dynamic-update-slice_fusion.1
  19.4 1.3 dynamic-update-slice.1
  20.7 43.7 %all-reduce.4 = (f32[16]{0:T(128)S(1)}, f32[16]{0:T(128)S(1)}) all-reduce(f32[16]{0:T(128)S(1)} %bitcast_dynamic-update-slice_fusion.1, f32[16]{0:T(128)S(1)} %dynamic-update-slice.1), channel_id=1, replica_groups=mesh['sp'=16,'tp'=2] {'sp'}, use_global_device_ids=true, to_apply=%add | all-reduce | flops 32 | bytes 256
  64.5 35.5 %all-gather.5 = f32[16,1,128]{2,1,0:T(1,128)S(1)} all-gather(f32[1,1,128]{2,1,0:T(1,128)S(1)} %multiply_bitcast_fusion), channel_id=3, replica_groups=mesh['sp'=16,'tp'=2] {'sp'}, dimensions={0}, use_global_device_ids=true | all-gather | bytes 8704 | tf_op jit(solution)/shard_map/all_gather | solution.py:14
  100.1 0.8 fusion.27
  102.6 1.3 convolution_bitcast_fusion
  104.0 0.9 fusion.36
  104.9 1.7 fusion.49
  106.6 0.7 copy.39
  107.4 2.0 subtract_dynamic-update-slice_fusion
  109.3 93.0 %all-reduce.2 = f32[16]{0:T(128)S(1)} all-reduce(f32[16]{0:T(128)S(1)} %subtract_dynamic-update-slice_fusion), channel_id=5, replica_groups=mesh['sp'=16,'tp'=2] {'sp'}, use_global_device_ids=true, to_apply=%add.2 | all-reduce | flops 16 | bytes 128
  202.4 35.5 %all-gather.6 = f32[16,1,128]{2,1,0:T(1,128)S(1)} all-gather(f32[1,1,128]{2,1,0:T(1,128)S(1)} %convolution_bitcast_fusion.7), channel_id=6, replica_groups=mesh['sp'=16,'tp'=2] {'sp'}, dimensions={0}, use_global_device_ids=true | all-gather | bytes 8704 | tf_op jit(solution)/shard_map/all_gather | solution.py:14
  238.8 1.6 copy.42
  240.4 54.7 %all-gather.12.cloned.1.call-done = f32[2048,256]{1,0:T(8,128)} async-done(((f32[128,256]{1,0:T(8,128)}), f32[2048,256]{1,0:T(8,128)}) %all-gather.12.cloned.1.call-update) | async-done | bytes 2097168 | tf_op jit(solution)/shard_map/all_gather | solution.py:14
  295.1 43.1 %while.45 = (s32[]{:T(128)}, f32[1,128,256]{2,1,0:T(8,128)S(1)}, f32[1,128]{1,0:T(1,128)S(1)}, s32[]{:T(128)}, f32[16,1,128,256]{3,2,1,0:T(8,128)}, /*index=5*/f...) while((s32[]{:T(128)}, f32[1,128,256]{2,1,0:T(8,128)S(1)}, ...), condition=%wide.region_10.11_spmd, body=%wide.region_9.10_spmd.sunk | while | flops 65798 | bytes 394935 | solution.py:23
  295.7 1.6 bitcast_add_fusion.7
  297.3 0.7 fusion.83
  298.6 1.6 bitcast_add_fusion.7
  300.2 0.7 fusion.83
  301.5 1.6 bitcast_add_fusion.7
  303.1 0.7 fusion.83
  304.4 1.6 bitcast_add_fusion.7
  306.0 0.7 fusion.83
  307.2 1.6 bitcast_add_fusion.7
  310.1 1.6 bitcast_add_fusion.7
  313.0 1.6 bitcast_add_fusion.7
  315.9 1.6 bitcast_add_fusion.7
  318.7 1.6 bitcast_add_fusion.7
  321.6 1.6 bitcast_add_fusion.7
  324.5 1.6 bitcast_add_fusion.7
  327.4 1.6 bitcast_add_fusion.7
  330.2 1.6 bitcast_add_fusion.7
  333.1 1.6 bitcast_add_fusion.7
  336.0 1.6 bitcast_add_fusion.7
  339.6 0.7 slice.25
  340.2 1.4 bitcast_dynamic-update-slice_fusion
  341.6 36.6 %all-reduce.3 = f32[16]{0:T(128)S(1)} all-reduce(f32[16]{0:T(128)S(1)} %bitcast_dynamic-update-slice_fusion), channel_id=1, replica_groups=mesh['sp'=16,'tp'=2] {'sp'}, use_global_device_ids=true, to_apply=%add.3 | all-reduce | flops 16 | bytes 128
  378.2 18.9 %while.46 = (s32[]{:T(128)}, f32[1]{0:T(128)}, s32[]{:T(128)}, f32[16,1]{0,1:T(1,128)S(1)}, s32[]{:T(128)}, /*index=5*/s32[]{:T(128)}, s32[]{:T(128)}, s32[]{:T(128)}) while((s32[]{:T(128)}, f32[1]{0:T(128)}, s32[]{:T(128)}, f32[16,1]{0,1:T(1,128)S(1)}, s32[]{:T(128)}, /*index=5*/s32[]{:T(128)}, s32[]{:T(128)}, s32[]{:T(128)}) %tuple.109), condition=%wide.region_16.17_spmd, body=%wide.region_15.16_spmd.sunk | while | flops 7 | bytes 155 | solution.py:23
  397.4 0.8 copy.41
  398.2 0.7 copy.40
  398.9 1.3 add_add_fusion
  (103 shorter events, 31.2 us)
Async XLA Ops:
  7.2 95.4 %copy-start = (bf16[256,2048]{1,0:T(8,128)(2,1)S(1)}, bf16[256,2048]{1,0:T(8,128)(2,1)}, u32[]{:S(2)}) copy-start(bf16[256,2048]{1,0:T(8,128)(2,1)} %param.13) | copy-start | bytes 3145732
  7.2 93.8 %copy-start.3 = (bf16[256,128]{1,0:T(8,128)(2,1)S(1)}, bf16[256,128]{1,0:T(8,128)(2,1)}, u32[]{:S(2)}) copy-start(bf16[256,128]{1,0:T(8,128)(2,1)} %param.15) | copy-start | bytes 196612
  7.2 93.8 %copy-start.5 = (f32[1,256]{1,0:T(1,128)S(1)}, f32[1,256]{1,0:T(1,128)}, u32[]{:S(2)}) copy-start(f32[1,256]{1,0:T(1,128)} %param.17) | copy-start | bytes 3076
  7.2 93.8 %copy-start.1 = (bf16[256,128]{1,0:T(8,128)(2,1)S(1)}, bf16[256,128]{1,0:T(8,128)(2,1)}, u32[]{:S(2)}) copy-start(bf16[256,128]{1,0:T(8,128)(2,1)} %param.14) | copy-start | bytes 196612
  7.2 93.7 %all-gather.10.cloned.1.call-start = ((), (), s32[]{:S(2)}) async-start(), calls=%async_computation.2 | async-start | bytes 2228224 | tf_op jit(solution)/shard_map/all_gather | solution.py:14
  12.9 88.5 %copy-start.2 = (bf16[256,256]{1,0:T(8,128)(2,1)S(1)}, bf16[256,256]{1,0:T(8,128)(2,1)}, u32[]{:S(2)}) copy-start(bf16[256,256]{1,0:T(8,128)(2,1)} %param.16) | copy-start | bytes 393220
  14.7 224.1 %reduce-scatter.2.cloned.1.call-start = ((), (), s32[]{:S(2)}) async-start(), calls=%async_computation.1 | async-start | bytes 1114112 | tf_op jit(solution)/shard_map/reduce_scatter | solution.py:137
  103.9 191.2 %all-gather.12.cloned.1.call-start = ((), (), s32[]{:S(2)}) async-start(), calls=%async_computation.3 | async-start | bytes 2228224 | tf_op jit(solution)/shard_map/all_gather | solution.py:14
  338.8 61.4 %copy-start.4 = (f32[256]{0:T(256)}, f32[256]{0:T(256)S(1)}, u32[]{:S(2)}) copy-start(f32[256]{0:T(256)S(1)} %get-tuple-element.373) | copy-start | bytes 3076
Sparse Core Ops, SparseCore 0:
  14.9 63.2 all-gather.9
  104.1 130.8 reduce-scatter.1
  238.3 56.7 all-gather.11
where the time goes:
time: 408 us; the launch traced here: 407 us
  blocking collectives  244 us (60%)
  waiting for transfers between devices  54.8 us (13%)
  other arithmetic  44.7 us (11%)
  local copies, waits for them, and re-layouts  31.5 us (8%)
  between operations  14.1 us (3%)
  loops' own time  10.6 us (3%)
  matrix products  6.66 us (2%)
    unnamed x3, blocking collectives  173 us
    all_gather x2, blocking collectives, carried_in(): gathered = jax.tree.map(lambda a: lax.all_gather(a, axis), part)  71 us
    all_gather x2, waiting for transfers between devices, carried_in(): gathered = jax.tree.map(lambda a: lax.all_gather(a, axis), part)  54.7 us
    add x15, other arithmetic, join_back(): latter_mat + keep_factor[:, None, None] * earlier_mat  23.9 us
    unnamed x27, local copies, waits for them, and re-layouts  12 us
    another operation x3, loops' own time, carried_in(): return lax.fori_loop(0, ahead, one, state)  10.6 us
    add x15, other arithmetic, join_back(): latter_vec + keep_factor[:, None] * earlier_vec  9.9 us
    exp x15, local copies, waits for them, and re-layouts, join_back(): keep_factor = jnp.exp(latter_decay)  8.88 us
  transfers between devices with their start and end apart: 3, of which 1 were waited for; matrix products, arithmetic and copies ran while one was open for 4% of the time, Pallas kernels for 0%

commit v1 on v0

v1 whole, which is shorter than its diff:
```python
import functools

import jax
import jax.numpy as jnp
from jax import lax
from jax.experimental import pallas as pl
from jax.experimental.pallas import tpu as pltpu
from jax.sharding import PartitionSpec as P

VERY_LOW = -1e30
F32 = jnp.float32
BF16 = jnp.bfloat16
LANES = 128
SUBLANES = 8
UNROLLED = 32


def nn(a, b):
    return lax.dot_general(a, b, (((1,), (0,)), ((), ())), preferred_element_type=F32)


def nt(a, b):
    return lax.dot_general(a, b, (((1,), (1,)), ((), ())), preferred_element_type=F32)


def tn(a, b):
    return lax.dot_general(a, b, (((0,), (0,)), ((), ())), preferred_element_type=F32)


def thirds(a):
    high = a.astype(BF16)
    rest = a - high.astype(F32)
    middle = rest.astype(BF16)
    return high, middle, (rest - middle.astype(F32)).astype(BF16)


def loop(count, body, init):
    if count <= UNROLLED:
        for i in range(count):
            init = body(i, init)
        return init
    return lax.fori_loop(0, count, body, init)


def each(count, body):
    def one(i, carry):
        body(i)
        return carry

    loop(count, one, 0)


def side_tile(rows_of, size):
    row = lax.broadcasted_iota(jnp.int32, (LANES, size), 0)
    tile = jnp.zeros((LANES, size), F32)
    for i, value in enumerate(rows_of):
        tile = jnp.where(row == i, value, tile)
    return tile.T


def kernel(
    n, inner,
    b_ref, q_ref, k_ref, v_ref, gate_ref, forget_ref, g_ref,
    gq_ref, gk_ref, gv_ref, gg_ref, gf_ref, gw_ref,
    bt_ref, seg_ref, seg_in, ent_out, ent_in,
    back_ref, back_in, lea_out, lea_in,
    part_ref, plane_in, plane_out, line_in, tail_ref, tail_in,
    seg_s, seg_r, ent_s, ent_r, back_s, back_r, lea_s, lea_r,
    plane_s, plane_r, line_s, line_r, tail_s, tail_r,
):
    me = lax.axis_index("sp")
    outer = n // inner
    my_out, my_in = me // inner, lax.rem(me, inner)
    owners, rows = ent_in.shape[0], ent_in.shape[1]
    length, dk = q_ref.shape
    dv = v_ref.shape[1]
    share = gw_ref.shape[0]
    sigma = dk ** (-0.5)

    def copy(src, dst, send, recv, device):
        return pltpu.make_async_remote_copy(
            src_ref=src, dst_ref=dst, send_sem=send, recv_sem=recv,
            device_id={"sp": device}, device_id_type=pl.DeviceIdType.MESH,
        )

    barrier = pltpu.get_barrier_semaphore()

    def greet(i):
        @pl.when(i != me)
        def _():
            pl.semaphore_signal(
                barrier, inc=1, device_id={"sp": i}, device_id_type=pl.DeviceIdType.MESH
            )

    each(n, greet)

    at_row = lax.broadcasted_iota(jnp.int32, (length, length), 0)
    at_col = lax.broadcasted_iota(jnp.int32, (length, length), 1)

    def to_col(row):
        return jnp.sum(jnp.where(at_row == at_col, row, 0.0), axis=1, keepdims=True)

    def to_row(col):
        return jnp.sum(jnp.where(at_row == at_col, col, 0.0), axis=0, keepdims=True)

    queries, keys, values, grads = q_ref[...], k_ref[...], v_ref[...], g_ref[...]
    broad_query, broad_key = queries.astype(F32), keys.astype(F32)
    gate = gate_ref[...]
    forget = forget_ref[...]
    sum_col = jnp.sum(jnp.where(at_col <= at_row, forget, 0.0), axis=1, keepdims=True)
    sum_row = to_row(sum_col)
    total = sum_row[:, length - 1:]
    tail_row = total - sum_row + gate
    seg_max = jnp.max(tail_row, axis=1, keepdims=True)
    tail_col = to_col(tail_row)
    weighted = (broad_key * jnp.exp(tail_col - seg_max)).astype(BF16)
    seg_vec = sigma * jnp.sum(weighted.astype(F32), axis=0, keepdims=True)
    seg_ref[:, :dv] = sigma * tn(weighted, values)
    seg_ref[:, dv:] = side_tile((seg_vec, total, seg_max), dk)

    def give(buffer, arrived, send, recv):
        def one(i):
            @pl.when(i != me)
            def _():
                copy(
                    buffer.at[pl.ds(i * rows, rows)], arrived.at[me], send.at[i], recv.at[me], i
                ).start()

            @pl.when(i == me)
            def _():
                arrived[me] = buffer[pl.ds(i * rows, rows)]

        each(owners, one)

    def given(buffer, arrived, send, recv):
        def one(i):
            @pl.when(i != me)
            def _():
                copy(
                    buffer.at[pl.ds(i * rows, rows)], arrived.at[me], send.at[i], recv.at[me], i
                ).wait_send()

        each(owners, one)

    def await_part(buffer, arrived, send, recv, i):
        @pl.when(i != me)
        def _():
            copy(
                buffer.at[pl.ds(0, rows)], arrived.at[i], send.at[0], recv.at[i], i
            ).wait_recv()

    def hand(state_ref, arrived, send, recv, j):
        @pl.when(j != me)
        def _():
            copy(state_ref.at[j], arrived.at[me], send.at[j], recv.at[me], j).start()

        @pl.when(j == me)
        def _():
            arrived[me] = state_ref[j]

    def handed(state_ref, arrived, send, recv):
        def one(j):
            @pl.when(j != me)
            def _():
                copy(state_ref.at[j], arrived.at[me], send.at[j], recv.at[me], j).wait_send()

        each(n, one)

    def collect(state_ref, arrived, send, recv):
        def one(i):
            @pl.when(i != me)
            def _():
                copy(state_ref.at[0], arrived.at[i], send.at[0], recv.at[i], i).wait_recv()

        each(owners, one)
        return arrived[...].reshape(owners * rows, arrived.shape[2])

    pl.semaphore_wait(barrier, n - 1)
    give(seg_ref, seg_in, seg_s, seg_r)

    at_wide = lax.broadcasted_iota(jnp.int32, (rows, dv + LANES), 1)
    causal = at_col <= at_row
    log_intra = jnp.where(causal, sum_col - sum_row + gate, -jnp.inf)
    intra_max = jnp.max(log_intra, axis=1, keepdims=True)
    scores = sigma * nt(queries, keys)

    def owner_forward():
        def one(j, carry):
            run_max, state = carry
            ent_out[j] = jnp.where(at_wide == dv + 1, run_max, state)
            hand(ent_out, ent_in, ent_s, ent_r, j)
            await_part(seg_ref, seg_in, seg_s, seg_r, j)
            fresh = seg_in[j]
            decayed = fresh[:, dv + 1:dv + 2] + run_max
            top = fresh[:, dv + 2:dv + 3]
            new_max = jnp.maximum(decayed, top)
            state = jnp.exp(decayed - new_max) * state + jnp.exp(top - new_max) * fresh
            return new_max, state

        loop(n, one, (jnp.full((rows, 1), VERY_LOW, F32), jnp.zeros((rows, dv + LANES), F32)))

    if owners == n:
        owner_forward()
    else:
        pl.when(me < owners)(owner_forward)

    bt_ref[...] = b_ref[...].T

    entered = collect(ent_out, ent_in, ent_s, ent_r)
    enter_side = entered[:, dv:].T
    enter_vec = enter_side[0:1]
    enter_max = enter_side[1:2, 0:1]
    enter_low = entered[:, :dv].astype(BF16)

    log_inter = sum_col + enter_max
    row_max = jnp.maximum(log_inter, intra_max)
    inter = jnp.exp(log_inter - row_max)
    intra = jnp.exp(log_intra - row_max)
    weighted_scores = intra * scores
    score_low = weighted_scores.astype(BF16)
    numerator = inter * nn(queries, enter_low) + nn(score_low, values)
    denominator = inter * jnp.sum(broad_query * enter_vec, axis=1, keepdims=True) + jnp.sum(
        weighted_scores, axis=1, keepdims=True
    )
    floor_scale = jnp.sqrt(denominator * denominator + jnp.exp(-2.0 * row_max))
    broad_grad = grads.astype(F32)
    delta_low = (broad_grad / floor_scale).astype(BF16)
    epsilon = (
        -jnp.sum(broad_grad * numerator, axis=1, keepdims=True)
        * denominator
        / (floor_scale * floor_scale * floor_scale)
    )
    leave_max = jnp.maximum(total + enter_max, seg_max)
    decay = total + enter_max - leave_max
    inter_query = inter * broad_query
    back_ref[:, :dv] = tn(inter_query.astype(BF16), delta_low)
    back_vec = jnp.sum(epsilon * inter_query, axis=0, keepdims=True)
    back_ref[:, dv:] = side_tile((back_vec, decay), dk)
    errors = nt(delta_low, values) + epsilon
    back_low = (intra * errors).astype(BF16)
    give(back_ref, back_in, back_s, back_r)

    grad_query = sigma * nn(back_low, keys) + inter * (
        nt(delta_low, enter_low) + epsilon * enter_vec
    )
    query_low = grad_query.astype(BF16)
    gq_ref[...] = query_low
    row_part = jnp.sum(broad_query * grad_query, axis=1, keepdims=True)
    part_ref[...] = nn(bt_ref[...], query_low)

    order = sorted(range(1, outer), key=lambda k: abs(2 * k - outer)) + [0]

    def plane_copy(far, p):
        return copy(
            part_ref.at[pl.ds((far * inner + p) * share, share)], plane_in.at[far, my_in],
            plane_s.at[far, p], plane_r.at[far, my_in], my_out * inner + p,
        )

    def plane_arrival(far, p):
        return copy(
            part_ref.at[pl.ds(0, share)], plane_in.at[far, p],
            plane_s.at[far, p], plane_r.at[far, p], my_out * inner + p,
        )

    for k in order:
        far = lax.rem(my_out + k, outer)

        for step in range(1, inner):
            plane_copy(far, lax.rem(my_in + step, inner)).start()

    key_intra = sigma * tn(back_low, queries)
    value_intra = tn(score_low, delta_low)
    key_decay = sigma * jnp.exp(tail_col - leave_max)

    def owner_back():
        def one(lap, state):
            j = n - 1 - lap
            lea_out[j] = state
            hand(lea_out, lea_in, lea_s, lea_r, j)
            await_part(back_ref, back_in, back_s, back_r, j)
            fresh = back_in[j]
            return fresh + jnp.exp(fresh[:, dv + 1:dv + 2]) * state

        loop(n, one, jnp.zeros((rows, dv + LANES), F32))

    if owners == n:
        owner_back()
    else:
        pl.when(me < owners)(owner_back)

    def line_copy(far):
        return copy(
            plane_out.at[far], line_in.at[my_out], line_s.at[far], line_r.at[my_out],
            far * inner + my_in,
        )

    for k in order:
        far = lax.rem(my_out + k, outer)
        joined = part_ref[pl.ds((far * inner + my_in) * share, share)]
        for step in range(1, inner):
            source = lax.rem(my_in + step, inner)
            plane_arrival(far, source).wait_recv()
            joined = joined + plane_in[far, source]
        plane_out[far] = joined
        if k:
            line_copy(far).start()

    left = collect(lea_out, lea_in, lea_s, lea_r)
    leave_vec = left[:, dv:].T[0:1]
    pieces = thirds(left[:, :dv])
    from_values = nt(values, pieces[2]) + nt(values, pieces[1]) + nt(values, pieces[0])
    from_keys = nn(keys, pieces[2]) + nn(keys, pieces[1]) + nn(keys, pieces[0])
    grad_key = key_intra + key_decay * (from_values + leave_vec)
    gate_col = jnp.sum(broad_key * grad_key, axis=1, keepdims=True)
    forget_part = row_part - gate_col
    part_total = jnp.sum(forget_part, axis=0, keepdims=True)
    tail_ref[...] = jnp.broadcast_to(part_total, tail_ref.shape)
    gk_ref[...] = grad_key.astype(BF16)
    gg_ref[...] = to_row(gate_col)
    suffix = jnp.sum(jnp.where(at_row >= at_col, forget_part, 0.0), axis=0, keepdims=True)

    def tail_copy(i):
        return copy(tail_ref, tail_in.at[me], tail_s.at[i], tail_r.at[me], i)

    def tell(i):
        @pl.when(i < me)
        def _():
            tail_copy(i).start()

    each(n, tell)
    gv_ref[...] = (value_intra + key_decay * from_keys).astype(BF16)

    whole = plane_out[my_out]
    for k in order[:-1]:
        far = lax.rem(my_out + k, outer)
        copy(
            plane_out.at[far], line_in.at[far], line_s.at[far], line_r.at[far],
            far * inner + my_in,
        ).wait_recv()
        whole = whole + line_in[far]
    gw_ref[...] = whole

    tail_in[me] = jnp.zeros(tail_ref.shape, F32)

    def hear(i):
        @pl.when(i > me)
        def _():
            copy(tail_ref, tail_in.at[i], tail_s.at[i], tail_r.at[i], i).wait_recv()

        @pl.when(i < me)
        def _():
            tail_in[i] = jnp.zeros(tail_ref.shape, F32)

    each(n, hear)
    later = jnp.sum(tail_in[...], axis=0)
    gf_ref[...] = suffix + later[0:1, 0:1]

    given(seg_ref, seg_in, seg_s, seg_r)
    given(back_ref, back_in, back_s, back_r)

    def owner_end():
        handed(ent_out, ent_in, ent_s, ent_r)
        handed(lea_out, lea_in, lea_s, lea_r)

    if owners == n:
        owner_end()
    else:
        pl.when(me < owners)(owner_end)
    for k in order:
        far = lax.rem(my_out + k, outer)
        for step in range(1, inner):
            plane_copy(far, lax.rem(my_in + step, inner)).wait_send()
        if k:
            line_copy(far).wait_send()

    def told(i):
        @pl.when(i < me)
        def _():
            tail_copy(i).wait_send()

    each(n, told)


def on_device(n, block_input, queries, keys, values, in_gate, log_forget, grad_out):
    length, dk = queries.shape
    dv = values.shape[1]
    width = block_input.shape[1]
    rows = max(SUBLANES, dk // n)
    owners = dk // rows
    share = width // n
    inner = max(d for d in range(1, n + 1) if n % d == 0 and d * d <= n)
    outer = n // inner
    wide = dv + LANES
    tile = (SUBLANES, LANES)
    vmem = pl.BlockSpec(memory_space=pltpu.VMEM)
    dma = pltpu.SemaphoreType.DMA
    return pl.pallas_call(
        functools.partial(kernel, n, inner),
        out_shape=(
            jax.ShapeDtypeStruct((length, dk), BF16),
            jax.ShapeDtypeStruct((length, dk), BF16),
            jax.ShapeDtypeStruct((length, dv), BF16),
            jax.ShapeDtypeStruct((1, length), F32),
            jax.ShapeDtypeStruct((1, length), F32),
            jax.ShapeDtypeStruct((share, dk), F32),
        ),
        in_specs=[vmem] * 7,
        out_specs=(vmem,) * 6,
        scratch_shapes=[
            pltpu.VMEM((width, length), BF16),
            pltpu.VMEM((dk, wide), F32),
            pltpu.VMEM((n, rows, wide), F32),
            pltpu.VMEM((n, rows, wide), F32),
            pltpu.VMEM((owners, rows, wide), F32),
            pltpu.VMEM((dk, wide), F32),
            pltpu.VMEM((n, rows, wide), F32),
            pltpu.VMEM((n, rows, wide), F32),
            pltpu.VMEM((owners, rows, wide), F32),
            pltpu.VMEM((width, dk), F32),
            pltpu.VMEM((outer, inner, share, dk), F32),
            pltpu.VMEM((outer, share, dk), F32),
            pltpu.VMEM((outer, share, dk), F32),
            pltpu.VMEM(tile, F32),
            pltpu.VMEM((n,) + tile, F32),
            dma((owners,)), dma((n,)), dma((n,)), dma((owners,)),
            dma((owners,)), dma((n,)), dma((n,)), dma((owners,)),
            dma((outer, inner)), dma((outer, inner)), dma((outer,)), dma((outer,)),
            dma((n,)), dma((n,)),
        ],
        compiler_params=pltpu.CompilerParams(collective_id=0, has_side_effects=True),
    )(block_input, queries, keys, values, in_gate, log_forget, grad_out)


def solution(mesh):
    seq, both, gates = P("sp", None), P("sp", "tp"), P("tp", "sp")
    return jax.shard_map(
        functools.partial(on_device, mesh.shape["sp"]),
        mesh=mesh,
        in_specs=(seq, both, both, both, gates, gates, both),
        out_specs=(both, both, both, gates, gates, both),
        check_vma=False,
    )
```

time: 408 us -> 50.8 us (0.12)
  blocking collectives: 244 us -> 0 us
  waiting for transfers between devices: 54.8 us -> 0 us
  Pallas kernels: 0 us -> 45.2 us
  other arithmetic: 44.7 us -> 0 us
  local copies, waits for them, and re-layouts: 31.5 us -> 4.69 us
  between operations: 14.1 us -> 0.66 us
  loops' own time: 10.6 us -> 0 us
  matrix products: 6.66 us -> 0 us
    unnamed x3 -> x0, blocking collectives: 173 us -> none
    all_gather x2 -> x0, blocking collectives: 71 us -> none  [carried_in(): gathered = jax.tree.map(lambda a: lax.all_gather(a, axis), part)]
    all_gather x2 -> x0, waiting for transfers between devices: 54.7 us -> none  [carried_in(): gathered = jax.tree.map(lambda a: lax.all_gather(a, axis), part)]
    pallas_call x0 -> x1, Pallas kernels: none -> 45.2 us  [on_device(): pl.pallas_call(functools.partial(kernel, n, inner), out_shape=(jax.ShapeD...]
    add x31 -> x0, other arithmetic: 35.1 us -> none  [the longest x15 23.9 us: join_back(): latter_mat + keep_factor[:, None, None] * earlier_mat]
    another operation x3 -> x0, loops' own time: 10.6 us -> none  [carried_in(): return lax.fori_loop(0, ahead, one, state)]
    exp x15 -> x0, local copies, waits for them, and re-layouts: 8.88 us -> none  [join_back(): keep_factor = jnp.exp(latter_decay)]
    dynamic_slice x15 -> x0, local copies, waits for them, and re-layouts: 8.78 us -> none  [one(): lax.dynamic_index_in_dim(a, source, 0, False)]
  transfers between devices with their start and end apart: 3 -> 0, of which waited for: 1 -> 0; matrix products, arithmetic and copies ran while one was open for 4% -> 0% of each run, Pallas kernels for 0% -> 0%
where the time goes in v1:
time: 50.8 us; the launch traced here: 50.6 us
  Pallas kernels  45.2 us (89%)
  local copies, waits for them, and re-layouts  4.69 us (9%)
  between operations  0.66 us (1%)
    pallas_call x1, Pallas kernels, on_device(): pl.pallas_call(functools.partial(kernel, n, inner), out_shape=(jax.ShapeD...  45.2 us
    unnamed x16, local copies, waits for them, and re-layouts  4.69 us

profile of v1, /device:TPU:0, one launch (start us, length us, event | category | flops | bytes accessed | tf_op | source)
XLA Modules:
  0.0 50.6 jit_solution(2221268567751976667)
XLA Ops:
  0.6 45.2 %shard_map.118 = (bf16[256,128]{1,0:T(8,128)(2,1)}, bf16[256,128]{1,0:T(8,128)(2,1)}, bf16[256,256]{1,0:T(8,128)(2,1)}, f32[1,256]{1,0:T(1,128)}, f32[1,256]{1,0:T(1,128)}, /*index=5*/f32[128,128]{1,0:T(8,128)}) custom-call(bf16[256,2048]{1,0:T(8,128)(2,1)} %b_ref.1, bf16[256,128]{1,0:T(8,128)(2,1)} %q_ref.1, bf16[256,128]{1,0:T(8,128)(2,1)} %k_ref.1, ...), custom_call_target="tpu_custom_call" | custom-call | tf_op jit(solution)/shard_map/pallas_call | solution.py:397
  45.8 0.0 copy-start.2
  45.9 0.0 copy-start
  45.9 1.5 %copy.19 = bf16[256,128]{1,0:T(8,128)(2,1)} copy(bf16[256,128]{1,0:T(8,128)(2,1)} %get-tuple-element.12) | data formatting | bytes 131072
  47.4 0.0 copy-done.2
  47.4 0.6 %copy.20 = bf16[256,128]{1,0:T(8,128)(2,1)} copy(bf16[256,128]{1,0:T(8,128)(2,1)S(1)} %copy-done.2) | data formatting | bytes 131072
  48.0 0.0 copy-done
  48.0 0.0 copy-start.4
  48.0 0.0 copy-start.1
  48.0 0.7 %copy.21 = bf16[256,256]{1,0:T(8,128)(2,1)} copy(bf16[256,256]{1,0:T(8,128)(2,1)S(1)} %copy-done) | data formatting | bytes 262144
  48.7 0.0 copy-done.4
  48.7 0.0 copy-start.3
  48.7 0.6 %copy.22 = f32[1,256]{1,0:T(1,128)} copy(f32[1,256]{1,0:T(1,128)S(1)} %copy-done.4) | data formatting | bytes 2048
  49.3 0.1 copy-done.3
  49.4 0.6 %copy.23 = f32[1,256]{1,0:T(1,128)} copy(f32[1,256]{1,0:T(1,128)S(1)} %copy-done.3) | data formatting | bytes 2048
  49.9 0.0 copy-done.1
  49.9 0.6 %copy.24 = f32[128,128]{1,0:T(8,128)} copy(f32[128,128]{1,0:T(8,128)S(1)} %copy-done.1) | data formatting | bytes 131072
Async XLA Ops:
  45.8 1.5 %copy-start.2 = (bf16[256,128]{1,0:T(8,128)(2,1)S(1)}, bf16[256,128]{1,0:T(8,128)(2,1)}, u32[]{:S(2)}) copy-start(bf16[256,128]{1,0:T(8,128)(2,1)} %get-tuple-element.13) | copy-start | bytes 196612
  45.9 2.2 %copy-start = (bf16[256,256]{1,0:T(8,128)(2,1)S(1)}, bf16[256,256]{1,0:T(8,128)(2,1)}, u32[]{:S(2)}) copy-start(bf16[256,256]{1,0:T(8,128)(2,1)} %get-tuple-element.14) | copy-start | bytes 393220
  48.0 0.7 %copy-start.4 = (f32[1,256]{1,0:T(1,128)S(1)}, f32[1,256]{1,0:T(1,128)}, u32[]{:S(2)}) copy-start(f32[1,256]{1,0:T(1,128)} %get-tuple-element.15) | copy-start | bytes 3076
  48.0 1.9 %copy-start.1 = (f32[128,128]{1,0:T(8,128)S(1)}, f32[128,128]{1,0:T(8,128)}, u32[]{:S(2)}) copy-start(f32[128,128]{1,0:T(8,128)} %get-tuple-element.17) | copy-start | bytes 196612
  48.7 0.7 %copy-start.3 = (f32[1,256]{1,0:T(1,128)S(1)}, f32[1,256]{1,0:T(1,128)}, u32[]{:S(2)}) copy-start(f32[1,256]{1,0:T(1,128)} %get-tuple-element.16) | copy-start | bytes 3076

commit v2 on v1

--- a/solution.py
+++ b/solution.py
@@ -64,9 +64,9 @@
     gq_ref, gk_ref, gv_ref, gg_ref, gf_ref, gw_ref,
     bt_ref, seg_ref, seg_in, ent_out, ent_in,
     back_ref, back_in, lea_out, lea_in,
-    part_ref, plane_in, plane_out, line_in, tail_ref, tail_in,
+    part_ref, plane_in, plane_out, line_in,
     seg_s, seg_r, ent_s, ent_r, back_s, back_r, lea_s, lea_r,
-    plane_s, plane_r, line_s, line_r, tail_s, tail_r,
+    plane_s, plane_r, line_s, line_r, wide_ref, wide_s,
 ):
     me = lax.axis_index("sp")
     outer = n // inner
@@ -85,14 +85,36 @@
 
     barrier = pltpu.get_barrier_semaphore()
 
+    def others(body):
+        def one(k):
+            far = (k + 1) // 2
+            body(lax.rem(me + (n // 2 + (far if k % 2 else -far) if n <= UNROLLED else k + 1) + n, n))
+
+        each(n - 1, one)
+
     def greet(i):
-        @pl.when(i != me)
-        def _():
-            pl.semaphore_signal(
-                barrier, inc=1, device_id={"sp": i}, device_id_type=pl.DeviceIdType.MESH
-            )
-
-    each(n, greet)
+        pl.semaphore_signal(
+            barrier, inc=1, device_id={"sp": i}, device_id_type=pl.DeviceIdType.MESH
+        )
+
+    others(greet)
+    fetch = pltpu.make_async_copy(b_ref, wide_ref, wide_s)
+    fetch.start()
+
+    def other_owners(body):
+        def one(i):
+            if owners == n:
+                body(i)
+            else:
+                pl.when(i < owners)(lambda: body(i))
+
+        others(one)
+
+    def as_owner(body):
+        if owners == n:
+            body()
+        else:
+            pl.when(me < owners)(body)
 
     at_row = lax.broadcasted_iota(jnp.int32, (length, length), 0)
     at_col = lax.broadcasted_iota(jnp.int32, (length, length), 1)
@@ -118,61 +140,49 @@
     seg_ref[:, :dv] = sigma * tn(weighted, values)
     seg_ref[:, dv:] = side_tile((seg_vec, total, seg_max), dk)
 
+    def give_copy(buffer, arrived, send, recv, i):
+        start = pl.multiple_of(i * rows, rows)
+        return copy(buffer.at[pl.ds(start, rows)], arrived.at[me], send.at[i], recv.at[me], i)
+
     def give(buffer, arrived, send, recv):
-        def one(i):
-            @pl.when(i != me)
-            def _():
-                copy(
-                    buffer.at[pl.ds(i * rows, rows)], arrived.at[me], send.at[i], recv.at[me], i
-                ).start()
-
-            @pl.when(i == me)
-            def _():
-                arrived[me] = buffer[pl.ds(i * rows, rows)]
-
-        each(owners, one)
+        other_owners(lambda i: give_copy(buffer, arrived, send, recv, i).start())
+
+        def own():
+            arrived[me] = buffer[pl.ds(pl.multiple_of(me * rows, rows), rows)]
+
+        as_owner(own)
 
     def given(buffer, arrived, send, recv):
-        def one(i):
-            @pl.when(i != me)
-            def _():
-                copy(
-                    buffer.at[pl.ds(i * rows, rows)], arrived.at[me], send.at[i], recv.at[me], i
-                ).wait_send()
-
-        each(owners, one)
-
-    def await_part(buffer, arrived, send, recv, i):
-        @pl.when(i != me)
-        def _():
-            copy(
+        other_owners(lambda i: give_copy(buffer, arrived, send, recv, i).wait_send())
+
+    def await_parts(buffer, arrived, send, recv):
+        others(
+            lambda i: copy(
                 buffer.at[pl.ds(0, rows)], arrived.at[i], send.at[0], recv.at[i], i
             ).wait_recv()
-
-    def hand(state_ref, arrived, send, recv, j):
-        @pl.when(j != me)
-        def _():
-            copy(state_ref.at[j], arrived.at[me], send.at[j], recv.at[me], j).start()
-
-        @pl.when(j == me)
-        def _():
-            arrived[me] = state_ref[j]
+        )
+
+    def hand(state_ref, arrived, send, recv):
+        others(
+            lambda j: copy(
+                state_ref.at[j], arrived.at[me], send.at[j], recv.at[me], j
+            ).start()
+        )
+        arrived[me] = state_ref[me]
 
     def handed(state_ref, arrived, send, recv):
-        def one(j):
-            @pl.when(j != me)
-            def _():
-                copy(state_ref.at[j], arrived.at[me], send.at[j], recv.at[me], j).wait_send()
-
-        each(n, one)
+        others(
+            lambda j: copy(
+                state_ref.at[j], arrived.at[me], send.at[j], recv.at[me], j
+            ).wait_send()
+        )
 
     def collect(state_ref, arrived, send, recv):
-        def one(i):
-            @pl.when(i != me)
-            def _():
-                copy(state_ref.at[0], arrived.at[i], send.at[0], recv.at[i], i).wait_recv()
-
-        each(owners, one)
+        other_owners(
+            lambda i: copy(
+                state_ref.at[0], arrived.at[i], send.at[0], recv.at[i], i
+            ).wait_recv()
+        )
         return arrived[...].reshape(owners * rows, arrived.shape[2])
 
     pl.semaphore_wait(barrier, n - 1)
@@ -185,11 +195,11 @@
     scores = sigma * nt(queries, keys)
 
     def owner_forward():
+        await_parts(seg_ref, seg_in, seg_s, seg_r)
+
         def one(j, carry):
             run_max, state = carry
             ent_out[j] = jnp.where(at_wide == dv + 1, run_max, state)
-            hand(ent_out, ent_in, ent_s, ent_r, j)
-            await_part(seg_ref, seg_in, seg_s, seg_r, j)
             fresh = seg_in[j]
             decayed = fresh[:, dv + 1:dv + 2] + run_max
             top = fresh[:, dv + 2:dv + 3]
@@ -198,13 +208,11 @@
             return new_max, state
 
         loop(n, one, (jnp.full((rows, 1), VERY_LOW, F32), jnp.zeros((rows, dv + LANES), F32)))
-
-    if owners == n:
-        owner_forward()
-    else:
-        pl.when(me < owners)(owner_forward)
-
-    bt_ref[...] = b_ref[...].T
+        hand(ent_out, ent_in, ent_s, ent_r)
+
+    as_owner(owner_forward)
+    fetch.wait()
+    bt_ref[...] = wide_ref[...].T
 
     entered = collect(ent_out, ent_in, ent_s, ent_r)
     enter_side = entered[:, dv:].T
@@ -232,6 +240,7 @@
     )
     leave_max = jnp.maximum(total + enter_max, seg_max)
     decay = total + enter_max - leave_max
+    leaving = jnp.exp(decay) * entered + jnp.exp(seg_max - leave_max) * seg_ref[...]
     inter_query = inter * broad_query
     back_ref[:, :dv] = tn(inter_query.astype(BF16), delta_low)
     back_vec = jnp.sum(epsilon * inter_query, axis=0, keepdims=True)
@@ -262,31 +271,30 @@
             plane_s.at[far, p], plane_r.at[far, p], my_out * inner + p,
         )
 
-    for k in order:
-        far = lax.rem(my_out + k, outer)
-
-        for step in range(1, inner):
-            plane_copy(far, lax.rem(my_in + step, inner)).start()
+    def plane_start(turns):
+        for k in turns:
+            for step in range(1, inner):
+                plane_copy(lax.rem(my_out + k, outer), lax.rem(my_in + step, inner)).start()
+
+    plane_start(order)
 
     key_intra = sigma * tn(back_low, queries)
     value_intra = tn(score_low, delta_low)
     key_decay = sigma * jnp.exp(tail_col - leave_max)
 
     def owner_back():
+        await_parts(back_ref, back_in, back_s, back_r)
+
         def one(lap, state):
             j = n - 1 - lap
             lea_out[j] = state
-            hand(lea_out, lea_in, lea_s, lea_r, j)
-            await_part(back_ref, back_in, back_s, back_r, j)
             fresh = back_in[j]
             return fresh + jnp.exp(fresh[:, dv + 1:dv + 2]) * state
 
         loop(n, one, jnp.zeros((rows, dv + LANES), F32))
-
-    if owners == n:
-        owner_back()
-    else:
-        pl.when(me < owners)(owner_back)
+        hand(lea_out, lea_in, lea_s, lea_r)
+
+    as_owner(owner_back)
 
     def line_copy(far):
         return copy(
@@ -313,21 +321,14 @@
     grad_key = key_intra + key_decay * (from_values + leave_vec)
     gate_col = jnp.sum(broad_key * grad_key, axis=1, keepdims=True)
     forget_part = row_part - gate_col
-    part_total = jnp.sum(forget_part, axis=0, keepdims=True)
-    tail_ref[...] = jnp.broadcast_to(part_total, tail_ref.shape)
     gk_ref[...] = grad_key.astype(BF16)
     gg_ref[...] = to_row(gate_col)
     suffix = jnp.sum(jnp.where(at_row >= at_col, forget_part, 0.0), axis=0, keepdims=True)
 
-    def tail_copy(i):
-        return copy(tail_ref, tail_in.at[me], tail_s.at[i], tail_r.at[me], i)
-
-    def tell(i):
-        @pl.when(i < me)
-        def _():
-            tail_copy(i).start()
-
-    each(n, tell)
+    at_side = lax.broadcasted_iota(jnp.int32, left.shape, 1)
+    pairing = jnp.where(at_side <= dv, left * leaving, 0.0)
+    later = jnp.sum(jnp.sum(pairing, axis=1, keepdims=True), axis=0, keepdims=True)
+    gf_ref[...] = suffix + later
     gv_ref[...] = (value_intra + key_decay * from_keys).astype(BF16)
 
     whole = plane_out[my_out]
@@ -340,21 +341,6 @@
         whole = whole + line_in[far]
     gw_ref[...] = whole
 
-    tail_in[me] = jnp.zeros(tail_ref.shape, F32)
-
-    def hear(i):
-        @pl.when(i > me)
-        def _():
-            copy(tail_ref, tail_in.at[i], tail_s.at[i], tail_r.at[i], i).wait_recv()
-
-        @pl.when(i < me)
-        def _():
-            tail_in[i] = jnp.zeros(tail_ref.shape, F32)
-
-    each(n, hear)
-    later = jnp.sum(tail_in[...], axis=0)
-    gf_ref[...] = suffix + later[0:1, 0:1]
-
     given(seg_ref, seg_in, seg_s, seg_r)
     given(back_ref, back_in, back_s, back_r)
 
@@ -362,10 +348,7 @@
         handed(ent_out, ent_in, ent_s, ent_r)
         handed(lea_out, lea_in, lea_s, lea_r)
 
-    if owners == n:
-        owner_end()
-    else:
-        pl.when(me < owners)(owner_end)
+    as_owner(owner_end)
     for k in order:
         far = lax.rem(my_out + k, outer)
         for step in range(1, inner):
@@ -373,12 +356,17 @@
         if k:
             line_copy(far).wait_send()
 
-    def told(i):
-        @pl.when(i < me)
-        def _():
-            tail_copy(i).wait_send()
-
-    each(n, told)
+
+def settle(*refs):
+    half = len(refs) // 2
+    sems = refs[-1]
+    moves = [
+        pltpu.make_async_copy(refs[i], refs[half + i], sems.at[i]) for i in range(half)
+    ]
+    for move in moves:
+        move.start()
+    for move in moves:
+        move.wait()
 
 
 def on_device(n, block_input, queries, keys, values, in_gate, log_forget, grad_out):
@@ -391,20 +379,16 @@
     inner = max(d for d in range(1, n + 1) if n % d == 0 and d * d <= n)
     outer = n // inner
     wide = dv + LANES
-    tile = (SUBLANES, LANES)
     vmem = pl.BlockSpec(memory_space=pltpu.VMEM)
     dma = pltpu.SemaphoreType.DMA
-    return pl.pallas_call(
+    results = (
+        ((length, dk), BF16), ((length, dk), BF16), ((length, dv), BF16),
+        ((1, length), F32), ((1, length), F32), ((share, dk), F32),
+    )
+    held = pl.pallas_call(
         functools.partial(kernel, n, inner),
-        out_shape=(
-            jax.ShapeDtypeStruct((length, dk), BF16),
-            jax.ShapeDtypeStruct((length, dk), BF16),
-            jax.ShapeDtypeStruct((length, dv), BF16),
-            jax.ShapeDtypeStruct((1, length), F32),
-            jax.ShapeDtypeStruct((1, length), F32),
-            jax.ShapeDtypeStruct((share, dk), F32),
-        ),
-        in_specs=[vmem] * 7,
+        out_shape=tuple(pltpu.VMEM(*r) for r in results),
+        in_specs=[pl.BlockSpec(memory_space=pl.ANY)] + [vmem] * 6,
         out_specs=(vmem,) * 6,
         scratch_shapes=[
             pltpu.VMEM((width, length), BF16),
@@ -420,15 +404,21 @@
             pltpu.VMEM((outer, inner, share, dk), F32),
             pltpu.VMEM((outer, share, dk), F32),
             pltpu.VMEM((outer, share, dk), F32),
-            pltpu.VMEM(tile, F32),
-            pltpu.VMEM((n,) + tile, F32),
             dma((owners,)), dma((n,)), dma((n,)), dma((owners,)),
             dma((owners,)), dma((n,)), dma((n,)), dma((owners,)),
             dma((outer, inner)), dma((outer, inner)), dma((outer,)), dma((outer,)),
-            dma((n,)), dma((n,)),
+            pltpu.VMEM((length, width), BF16), dma,
         ],
         compiler_params=pltpu.CompilerParams(collective_id=0, has_side_effects=True),
     )(block_input, queries, keys, values, in_gate, log_forget, grad_out)
+    held = [pltpu.with_memory_space_constraint(h, pltpu.VMEM) for h in held]
+    return pl.pallas_call(
+        settle,
+        out_shape=tuple(jax.ShapeDtypeStruct(*r) for r in results),
+        in_specs=[vmem] * 6,
+        out_specs=(pl.BlockSpec(memory_space=pl.ANY),) * 6,
+        scratch_shapes=[dma((6,))],
+    )(*held)
 
 
 def solution(mesh):

time: 50.8 us -> 40.9 us (0.81)
  Pallas kernels: 45.2 us -> 40.1 us
  local copies, waits for them, and re-layouts: 4.69 us -> 0 us
    pallas_call x1 -> x2, Pallas kernels: 45.2 us -> 40.1 us  [the longest x1 39.3 us: on_device(): pl.pallas_call(functools.partial(kernel, n, inner), out_shape=tuple((pltp...]
    unnamed x16 -> x0, local copies, waits for them, and re-layouts: 4.69 us -> none
where the time goes in v2:
time: 40.9 us; the launch traced here: 40.8 us
  Pallas kernels  40.1 us (98%)
  between operations  0.64 us (2%)
    pallas_call x1, Pallas kernels, on_device(): pl.pallas_call(functools.partial(kernel, n, inner), out_shape=tuple((pltp...  39.3 us

profile of v2, /device:TPU:0, one launch (start us, length us, event | category | flops | bytes accessed | tf_op | source)
XLA Modules:
  0.0 40.8 jit_solution(10589682615298534931)
XLA Ops:
  0.6 39.3 %shard_map.118 = (bf16[256,128]{1,0:T(8,128)(2,1)S(1)}, bf16[256,128]{1,0:T(8,128)(2,1)S(1)}, bf16[256,256]{1,0:T(8,128)(2,1)S(1)}, f32[1,256]{1,0:T(1,128)S(1)}...) custom-call(bf16[256,2048]{1,0:T(8,128)(2,1)} %b_ref.1, bf16[256,128]{1,0:T(8,128)(2,1)} %q_ref.1, bf16[256,128]{1,0:T(8,128)(2,1)} %k_ref.1, ...), custom_call_target="tpu_custom_call" | custom-call | tf_op jit(solution)/shard_map/pallas_call | solution.py:388
  40.0 0.8 %shard_map.119 = (bf16[256,128]{1,0:T(8,128)(2,1)}, bf16[256,128]{1,0:T(8,128)(2,1)}, bf16[256,256]{1,0:T(8,128)(2,1)}, f32[1,256]{1,0:T(1,128)}, f32[1,256]{1,0:T(1,128)}, /*index=5*/f32[128,128]{1,0:T(8,128)}) custom-call(bf16[256,128]{1,0:T(8,128)(2,1)S(1)} %get-tuple-element.12.refs_0_, bf16[256,128]{1,0:T(8,128)(2,1)S(1)} %get-tuple-element.13.refs_1_, ...), custom_call_target="tpu_custom_call" | custom-call | tf_op jit(solution)/shard_map/pallas_call | solution.py:415
